TPU v7x, 32 devices: a whole 2x2x4 slice. The times are simulated.
32 devices in a mesh: ep: 8 (over z, x), tp: 4 (over y, core).
Axes of the slice: x: 2, y: 2, z: 4, core: 2. Of those that a mesh axis runs over, the one named last changes fastest.
Arguments:
- tokens: bfloat16 [64, 2048], P('ep'), may hold values from -6 to 6
- mix_gain: bfloat16 [2048], replicated, may hold values from 0.099609375 to 1.8984375
- w_query: bfloat16 [2048, 512], P(None, 'tp'), may hold values from -0.125 to 0.125
- w_key: bfloat16 [2048, 512], P(None, 'tp'), may hold values from -0.125 to 0.125
- w_value: bfloat16 [2048, 512], P(None, 'tp'), may hold values from -0.125 to 0.125
- w_igate: bfloat16 [2048, 4], replicated, may hold values from -0.125 to 0.125
- w_fgate: bfloat16 [2048, 4], replicated, may hold values from -0.125 to 0.125
- forget_bias: float32 [4], replicated, may hold values from 0.5 to 4.5
- w_out: bfloat16 [512, 2048], P('tp'), may hold values from -0.25 to 0.25
- mem_state: float32 [64, 4, 16384], P('ep', 'tp'), may hold values from -0.75 to 0.75
- norm_state: float32 [64, 512], P('ep', 'tp'), may hold values from -0.75 to 0.75
- max_state: float32 [64, 4], P('ep', 'tp'), may hold values from -3 to 3
- ffn_gain: bfloat16 [2048], replicated, may hold values from 0.099609375 to 1.8984375
- route_ids: int32 [64, 2], P('ep'), may hold values from 0 to 7, all different within a row; in each aligned block of 8 rows (0 to 7, 8 to 15, ...) at most 3 rows name the same one
- route_weights: float32 [64, 2], P('ep'), may hold values from 0.1 to 1
- w_gate: bfloat16 [2048, 32768], P(None, ('ep', 'tp')), may hold values from -0.125 to 0.125
- w_up: bfloat16 [2048, 32768], P(None, ('ep', 'tp')), may hold values from -0.125 to 0.125
- w_down: bfloat16 [32768, 2048], P('ep', 'tp'), may hold values from -0.09375 to 0.09375
Outputs:
- out_tokens: bfloat16 [64, 2048], P('ep', 'tp')
- new_memory: float32 [64, 4, 16384], P('ep', 'tp')
- new_norm: float32 [64, 512], P('ep', 'tp')
- new_max: float32 [64, 4], P('ep', 'tp')
Inputs may be any that keep to these rules, and one draw needn't show every extreme that they name: `route_ids`: each row names 2 different experts; among the rows of one index of ep no expert is named more than 3 times, a bound that some block reaches.
All inputs are finite; a program needn't handle non-finite values.
Results may differ from a plain program's by a relative error of at most 0.013.
The roundings to bfloat16 on the way count: a program that leaves them out, or rounds other values in their place, can miss the bound.
Values may be sent and summed in bfloat16 or wider, within the bound.
A program may use at most 64 MiB of HBM per device.

v0:
```python
import jax
import jax.numpy as jnp
from jax import lax
from jax.sharding import PartitionSpec as P

FF = 4096


epsilon = 1e-06


def scaled_rows(row_data, squares, feature_count, gain_values):
    factor = lax.rsqrt(squares / feature_count + epsilon)
    return (row_data * factor[:, None] * gain_values.astype(jnp.float32)).astype(jnp.bfloat16)


def rounded_wide(matrix):
    return lax.optimization_barrier(matrix.astype(jnp.bfloat16)).astype(jnp.float32)


def shards(
    tokens,
    mix_gain,
    w_query,
    w_key,
    w_value,
    w_igate,
    w_fgate,
    forget_bias,
    w_out,
    mem_state,
    norm_state,
    max_state,
    ffn_gain,
    route_ids,
    route_weights,
    w_gate,
    w_up,
    w_down,
):
    seq_count, model_width = tokens.shape
    local_heads = mem_state.shape[1]
    head_dim = norm_state.shape[1] // local_heads
    tp_count = lax.axis_size("tp")
    tp_at = lax.axis_index("tp")
    ep_count = lax.axis_size("ep")
    own_width = model_width // tp_count
    top_count = route_ids.shape[1]
    block_units = w_down.shape[0]
    span_count = FF // block_units
    experts = ep_count // span_count
    slot_cap = max(2, 3 * seq_count * top_count // (2 * experts))
    residual_in = tokens.astype(jnp.float32)
    normed = scaled_rows(residual_in, jnp.sum(residual_in * residual_in, 1), model_width, mix_gain)

    def project(weight):
        product = jnp.dot(normed, weight, preferred_element_type=jnp.float32)
        return rounded_wide(product).reshape(seq_count, local_heads, head_dim)

    query_rows = project(w_query)
    key_rows = project(w_key) * head_dim ** (-0.5)
    value_rows = project(w_value)
    head_start = tp_at * local_heads
    input_gate = lax.dynamic_slice_in_dim(
        jnp.dot(normed, w_igate, preferred_element_type=jnp.float32), head_start, local_heads, 1
    )
    forget_pre = jnp.dot(normed, w_fgate, preferred_element_type=jnp.float32) + forget_bias[None, :]
    forget_log = jax.nn.log_sigmoid(
        lax.dynamic_slice_in_dim(forget_pre, head_start, local_heads, 1)
    )
    new_max = jnp.maximum(forget_log + max_state, input_gate)
    keep_weight = jnp.exp(forget_log + max_state - new_max)
    new_weight = jnp.exp(input_gate - new_max)
    memory = mem_state.reshape(seq_count, local_heads, head_dim, head_dim)
    new_memory = (
        keep_weight[:, :, None, None] * memory
        + new_weight[:, :, None, None] * key_rows[:, :, :, None] * value_rows[:, :, None, :]
    )
    new_norm = (
        keep_weight[:, :, None] * norm_state.reshape(seq_count, local_heads, head_dim)
        + new_weight[:, :, None] * key_rows
    )
    numerator = jnp.einsum("shd,shde->she", query_rows, new_memory, precision=lax.Precision.HIGHEST)
    denominator = jnp.sum(query_rows * new_norm, axis=2)
    readout = (numerator / jnp.maximum(jnp.abs(denominator), jnp.exp(-new_max))[:, :, None]).astype(
        jnp.bfloat16
    )
    readout = readout.reshape(seq_count, local_heads * head_dim)
    partial_value = jnp.dot(readout, w_out, preferred_element_type=jnp.float32)
    head_total = lax.psum(partial_value.astype(jnp.bfloat16), "tp").astype(jnp.float32)
    residual = (residual_in + head_total).astype(jnp.bfloat16)
    residual_wide = lax.optimization_barrier(residual).astype(jnp.float32)
    outgoing = scaled_rows(
        residual_wide, jnp.sum(residual_wide * residual_wide, 1), model_width, ffn_gain
    )
    own_residual = lax.dynamic_slice_in_dim(residual, tp_at * own_width, own_width, 1)
    flat_ids = route_ids.reshape(-1)
    matches = (flat_ids[:, None] == jnp.arange(experts, dtype=jnp.int32)[None, :]).astype(jnp.int32)
    slot_rank = jnp.sum((jnp.cumsum(matches, 0) - matches) * matches, 1)
    slot_index = (flat_ids * slot_cap + slot_rank).reshape(seq_count, top_count)
    chosen = (
        slot_index[:, :, None] == jnp.arange(experts * slot_cap, dtype=jnp.int32)[None, None, :]
    ).astype(jnp.float32)
    placing = jnp.sum(chosen, 1).astype(jnp.bfloat16)
    mixing = jnp.sum(chosen * route_weights[:, :, None], 1)
    packed = jnp.einsum("sj,sc->jc", placing, outgoing, preferred_element_type=jnp.float32).astype(
        jnp.bfloat16
    )
    packed_width = packed.shape[1]
    outbound = jnp.broadcast_to(
        packed.reshape(experts, 1, slot_cap, packed_width),
        (experts, span_count, slot_cap, packed_width),
    ).reshape(ep_count, slot_cap, packed_width)
    arrived = lax.all_to_all(outbound, "ep", split_axis=0, concat_axis=0, tiled=True)
    sources = arrived.shape[0]
    item_count = arrived.shape[1]
    flat_rows = arrived.reshape(sources * item_count, arrived.shape[2])
    gate_sum = jnp.dot(flat_rows, w_gate, preferred_element_type=jnp.float32)
    up_sum = jnp.dot(flat_rows, w_up, preferred_element_type=jnp.float32)
    hidden = (jax.nn.silu(gate_sum) * up_sum).astype(jnp.bfloat16)
    partial_out = jnp.dot(
        lax.all_gather(hidden, "tp", axis=1, tiled=True), w_down, preferred_element_type=jnp.float32
    )
    returned = lax.all_to_all(
        partial_out.reshape(sources, item_count, w_down.shape[1]).astype(jnp.bfloat16),
        "ep",
        split_axis=0,
        concat_axis=0,
        tiled=True,
    ).astype(jnp.float32)
    results = jnp.sum(returned.reshape(experts, span_count, slot_cap, own_width), 1).reshape(
        experts * slot_cap, own_width
    )
    routed = jnp.dot(
        mixing, results, precision=lax.Precision.HIGHEST, preferred_element_type=jnp.float32
    )
    out_tokens = (own_residual.astype(jnp.float32) + routed).astype(jnp.bfloat16)
    return (
        out_tokens,
        new_memory.reshape(seq_count, local_heads, head_dim * head_dim),
        new_norm.reshape(seq_count, local_heads * head_dim),
        new_max,
    )


def solution(mesh):
    placed = (
        P("ep", None),
        P(),
        P(None, "tp"),
        P(None, "tp"),
        P(None, "tp"),
        P(),
        P(),
        P(),
        P("tp", None),
        P("ep", "tp", None),
        P("ep", "tp"),
        P("ep", "tp"),
        P(),
        P("ep", None),
        P("ep", None),
        P(None, ("ep", "tp")),
        P(None, ("ep", "tp")),
        P("ep", "tp"),
    )
    return jax.shard_map(
        shards,
        mesh=mesh,
        in_specs=placed,
        out_specs=(P("ep", "tp"), P("ep", "tp", None), P("ep", "tp"), P("ep", "tp")),
        check_vma=False,
    )
```

profile of v0, /device:TPU:0, one launch (start us, length us, event | category | flops | bytes accessed | tf_op | source)
XLA Modules:
  0.0 65.1 jit_solution(17769218186569641081)
XLA Ops:
  0.6 0.0 copy-start
  0.6 0.9 %fusion.9 = f32[8]{0:T(128)S(1)} fusion(bf16[8,2048]{1,0:T(8,128)(2,1)} %param.18), kind=kLoop, calls=%fused_computation.25 | loop fusion | flops 49144 | bytes 32800 | tf_op jit(solution)/shard_map/reduce_sum | solution.py:54
  1.6 0.8 %copy.36 = s32[8,2]{1,0:T(8,128)S(1)} copy(s32[8,2]{0,1:T(2,128)} %param.31) | data formatting | bytes 128 | tf_op args[13]
  2.4 0.1 eq.28
  2.4 0.7 %copy.34 = f32[8,1]{1,0:T(8,128)S(1)} copy(f32[8,1]{0,1:T(1,128)} %param.29) | data formatting | bytes 64 | tf_op args[11]
  3.2 0.7 %convert_element_type.78 = f32[2048]{0:T(1024)S(1)} convert(bf16[2048]{0:T(1024)(128)(2,1)} %param.19) | non-fusion elementwise | flops 2048 | bytes 12288 | tf_op jit(solution)/shard_map/convert_element_type | solution.py:14
  3.9 1.3 %convolution_convert_fusion.4 = bf16[8,128]{1,0:T(8,128)(2,1)S(1)} fusion(bf16[2048,128]{1,0:T(8,128)(2,1)} %param.21, bf16[8,2048]{1,0:T(8,128)(2,1)} %param.18, f32[2048]{0:T(1024)S(1)} %convert_element_type.78, f32[8]{0:T(128)S(1)} %add_rsqrt_fusion.1), kind=kOutput, calls=%fused_computation.9 | convolution fusion | flops 4260864 | bytes 567328 | tf_op jit(solution)/shard_map/dot_general | solution.py:57
  5.2 1.3 %convolution_convert_fusion.3 = bf16[8,128]{1,0:T(8,128)(2,1)S(1)} fusion(bf16[2048,128]{1,0:T(8,128)(2,1)} %param.22, bf16[8,2048]{1,0:T(8,128)(2,1)} %param.18, f32[2048]{0:T(1024)S(1)} %convert_element_type.78, f32[8]{0:T(128)S(1)} %add_rsqrt_fusion.1), kind=kOutput, calls=%fused_computation.8 | convolution fusion | flops 4260864 | bytes 567328 | tf_op jit(solution)/shard_map/dot_general | solution.py:57
  6.5 1.3 %convolution_convert_fusion.5 = bf16[8,128]{1,0:T(8,128)(2,1)S(1)} fusion(bf16[2048,128]{1,0:T(8,128)(2,1)} %param.20, bf16[8,2048]{1,0:T(8,128)(2,1)} %param.18, f32[2048]{0:T(1024)S(1)} %convert_element_type.78, f32[8]{0:T(128)S(1)} %add_rsqrt_fusion.1), kind=kOutput, calls=%fused_computation.10 | convolution fusion | flops 4260864 | bytes 567328 | tf_op jit(solution)/shard_map/dot_general | solution.py:57
  7.8 1.0 %fusion.24 = f32[8,4]{1,0:T(8,128)S(1)} fusion(bf16[2048,4]{0,1:T(4,128)(2,1)} %param.23, bf16[8,2048]{1,0:T(8,128)(2,1)} %param.18, f32[2048]{0:T(1024)S(1)} %convert_element_type.78, f32[8]{0:T(128)S(1)} %add_rsqrt_fusion.1), kind=kOutput, calls=%fused_computation.55 | convolution fusion | flops 196608 | bytes 57504 | tf_op jit(solution)/shard_map/dot_general | solution.py:65
  8.7 1.0 %convolution_add_fusion.1 = f32[8,4]{1,0:T(8,128)S(1)} fusion(bf16[2048,4]{0,1:T(4,128)(2,1)} %param.24, f32[4]{0:T(128)} %param.25, bf16[8,2048]{1,0:T(8,128)(2,1)} %param.18, f32[2048]{0:T(1024)S(1)} %convert_element_type.78, f32[8]{0:T(128)S(1)} %add_rsqrt_fusion.1), kind=kOutput, calls=%fused_computation.7 | convolution fusion | flops 196640 | bytes 57520 | tf_op jit(solution)/shard_map/dot_general | solution.py:67
  9.7 0.2 multiply_reduce_fusion.1
  9.9 1.5 %multiply_reduce_fusion = (f32[8]{0:T(128)S(1)}, f32[8,128]{1,0:T(8,128)}, f32[8,128]{1,0:T(8,128)S(1)}) fusion(bf16[8,128]{1,0:T(8,128)(2,1)S(1)} %convolution_convert_fusion.5, f32[8]{0:T(128)S(1)} %get-tuple-element.16, bf16[8,128]{1,0:T(8,128)(2,1)S(1)} %convolution_convert_fusion.4, f32[8,128]{1,0:T(8,128)} %param.28, f32[8]{0:T(128)S(1)} %get-tuple-element.17), kind=kLoop, calls=%fused_computation.44 | loop fusion | flops 7160 | bytes 16480 | tf_op jit(solution)/shard_map/reduce_sum | solution.py:84
  11.4 0.1 copy.35
  11.5 0.1 fusion.16
  11.6 0.2 select_reduce_fusion.1
  11.8 0.1 reduce_sum.63
  11.9 0.1 copy.38
  12.0 0.7 %convert_element_type.95 = f32[2048]{0:T(1024)S(1)} convert(bf16[2048]{0:T(1024)(128)(2,1)} %param.30) | non-fusion elementwise | flops 2048 | bytes 12288 | tf_op jit(solution)/shard_map/convert_element_type | solution.py:14
  12.7 0.1 maximum_reduce_fusion
  12.8 1.5 %fusion.2 = f32[8,1,128]{2,1,0:T(1,128)S(1)} fusion(f32[8,128,128]{2,1,0:T(8,128)} %bitcast.22, f32[8]{0:T(128)S(1)} %get-tuple-element.17, f32[8,128]{1,0:T(8,128)S(1)} %convert_element_type.84, f32[8,128]{1,0:T(8,128)S(1)} %get-tuple-element.23, bf16[8,128,1]{1,0,2:T(8,128)(2,1)S(1)} %bitcast.24), kind=kOutput, calls=%fused_computation.12 | convolution fusion | flops 1966080 | bytes 538656 | tf_op jit(solution)/shard_map/shd,shde->she/dot_general | solution.py:83
  14.3 0.0 copy-done
  14.3 0.2 convolution_convert_fusion.1
  14.5 12.9 %psum.7 = bf16[8,2048]{1,0:T(8,128)(2,1)S(1)} all-reduce(bf16[8,2048]{1,0:T(8,128)(2,1)S(1)} %convolution_convert_fusion.1), channel_id=1, replica_groups=mesh['ep'=8,'tp'=4] {'tp'}, use_global_device_ids=true, to_apply=%region_2.3 | all-reduce | flops 16384 | bytes 65536 | tf_op jit(solution)/shard_map/psum | solution.py:90
  27.5 0.8 %fusion.12 = bf16[8,2048]{1,0:T(8,128)(2,1)S(1)} fusion(bf16[8,2048]{1,0:T(8,128)(2,1)} %param.18, bf16[8,2048]{1,0:T(8,128)(2,1)S(1)} %psum.7), kind=kLoop, calls=%fused_computation.28 | loop fusion | flops 65536 | bytes 98304 | tf_op jit(solution)/shard_map/convert_element_type | solution.py:91
  28.3 0.1 fusion.6
  28.4 0.8 %convert_reduce_fusion = (bf16[8,24]{1,0:T(8,128)(2,1)S(1)}, f32[8,24]{1,0:T(8,128)S(1)}) fusion(s32[8,2]{0,1:T(2,128)S(1)} %copy.38, f32[8,2]{0,1:T(2,128)} %param.32), kind=kLoop, calls=%fused_computation.32 | loop fusion | flops 1536 | bytes 1280 | tf_op jit(solution)/shard_map/reduce_sum | solution.py:104
  29.2 0.2 convolution_convert_fusion
  29.4 0.7 %reshape_reshape.3 = bf16[8,3,2048]{2,1,0:T(4,128)(2,1)} reshape(bf16[24,2048]{1,0:T(8,128)(2,1)S(1)} %convolution_convert_fusion) | data formatting | bytes 196608 | tf_op jit(solution)/shard_map/reshape;reshape | solution.py:113
  30.1 5.8 %all-to-all-start = ((bf16[8,3,2048]{2,1,0:T(4,128)(2,1)}), bf16[8,3,2048]{2,1,0:T(4,128)(2,1)S(1)}, u32[]{:S(2)}, u32[]{:S(2)}) async-start(bf16[8,3,2048]{2,1,0:T(4,128)(2,1)} %reshape_reshape.3), calls=%async_computation | async-start | bytes 262144 | tf_op jit(solution)/shard_map/all_to_all | solution.py:114
  35.9 0.2 broadcast_multiply_fusion
  36.1 7.1 %all-to-all-done = bf16[8,3,2048]{2,1,0:T(4,128)(2,1)S(1)} async-done(((bf16[8,3,2048]{2,1,0:T(4,128)(2,1)}), bf16[8,3,2048]{2,1,0:T(4,128)(2,1)S(1)}, u32[]{:S(2)}, u32[]{:S(2)}) %all-to-all-start) | async-done | bytes 98336 | tf_op jit(solution)/shard_map/all_to_all | solution.py:114
  43.3 0.1 reshape.138
  43.4 0.0 copy-start.1
  43.4 0.0 copy-start.2
  43.4 3.0 %fusion.28 = f32[24,1024]{1,0:T(8,128)S(1)} fusion(bf16[24,2048]{1,0:T(8,128)(2,1)S(1)} %reshape.138, bf16[2048,1024]{1,0:T(8,128)(2,1)} %param.33), kind=kOutput, calls=%fused_computation.56 | convolution fusion | flops 100663296 | bytes 4390912 | tf_op jit(solution)/shard_map/dot_general | solution.py:118
  46.4 0.4 copy-done.1
  46.8 0.7 %fusion = bf16[24,1024]{1,0:T(8,128)(2,1)S(1)} fusion(bf16[24,2048]{1,0:T(8,128)(2,1)S(1)} %reshape.138, bf16[2048,1024]{1,0:T(8,128)(2,1)S(1)} %copy-done.1, f32[24,1024]{1,0:T(8,128)S(1)} %fusion.28), kind=kOutput, calls=%fused_computation.3 | convolution fusion | flops 100810752 | bytes 4440064 | tf_op jit(solution)/shard_map/dot_general | solution.py:119
  47.5 5.6 %all_gather.3 = bf16[24,4096]{1,0:T(8,128)(2,1)S(1)} all-gather(bf16[24,1024]{1,0:T(8,128)(2,1)S(1)} %fusion), channel_id=1, replica_groups=mesh['ep'=8,'tp'=4] {'tp'}, dimensions={1}, use_global_device_ids=true | all-gather | bytes 245760 | tf_op jit(solution)/shard_map/all_gather | solution.py:122
  53.1 0.0 copy-done.2
  53.1 0.7 %convolution_convert_fusion.2 = bf16[24,512]{1,0:T(8,128)(2,1)S(1)} fusion(bf16[24,4096]{1,0:T(8,128)(2,1)S(1)} %all_gather.3, bf16[4096,512]{1,0:T(8,128)(2,1)S(1)} %copy-done.2), kind=kOutput, calls=%fused_computation.4 | convolution fusion | flops 100675584 | bytes 4415488 | tf_op jit(solution)/shard_map/dot_general | solution.py:121
  53.7 0.6 convert_element_type.100
  54.4 3.3 %all-to-all-start.1 = ((bf16[8,3,512]{2,1,0:T(4,128)(2,1)}), bf16[8,3,512]{2,1,0:T(4,128)(2,1)S(1)}, u32[]{:S(2)}, u32[]{:S(2)}) async-start(bf16[8,3,512]{2,1,0:T(4,128)(2,1)} %convert_element_type.100), calls=%async_computation.1 | async-start | bytes 65536 | tf_op jit(solution)/shard_map/all_to_all | solution.py:124
  57.7 0.0 copy-done.3
  57.7 1.4 %multiply_add_fusion = f32[8,1,16384]{2,1,0:T(1,128)} fusion(f32[8,1,16384]{2,1,0:T(1,128)S(1)} %bitcast.23, f32[8,1,16384]{2,1,0:T(1,128)S(1)} %copy-done.3, f32[8]{0:T(128)S(1)} %get-tuple-element.17), kind=kLoop, calls=%fused_computation.11 | loop fusion | flops 262144 | bytes 1572896 | tf_op jit(solution)/shard_map/add | solution.py:76
  59.1 0.6 copy.39
  59.7 4.6 %all-to-all-done.1 = bf16[8,3,512]{2,1,0:T(4,128)(2,1)S(1)} async-done(((bf16[8,3,512]{2,1,0:T(4,128)(2,1)}), bf16[8,3,512]{2,1,0:T(4,128)(2,1)S(1)}, u32[]{:S(2)}, u32[]{:S(2)}) %all-to-all-start.1) | async-done | bytes 24608 | tf_op jit(solution)/shard_map/all_to_all | solution.py:124
  64.4 0.7 %fusion.1 = bf16[8,512]{1,0:T(8,128)(2,1)} fusion(f32[8,24]{1,0:T(8,128)S(1)} %get-tuple-element.19, bf16[24,512]{1,0:T(8,128)(2,1)S(1)} %reshape.139, bf16[8,2048]{1,0:T(8,128)(2,1)S(1)} %fusion.12, s32[]{:T(128)S(6)} %select_n.14), kind=kOutput, calls=%fused_computation.6 | convolution fusion | flops 1191936 | bytes 41732 | tf_op jit(solution)/shard_map/dot_general | solution.py:134
  (8 shorter events, 0.1 us)
Async XLA Ops:
  0.6 13.7 %copy-start = (bf16[128,2048]{1,0:T(8,128)(2,1)S(1)}, bf16[128,2048]{1,0:T(8,128)(2,1)}, u32[]{:S(2)}) copy-start(bf16[128,2048]{1,0:T(8,128)(2,1)} %param.26) | copy-start | bytes 1572868
  30.1 13.1 %all-to-all-start = ((bf16[8,3,2048]{2,1,0:T(4,128)(2,1)}), bf16[8,3,2048]{2,1,0:T(4,128)(2,1)S(1)}, u32[]{:S(2)}, u32[]{:S(2)}) async-start(bf16[8,3,2048]{2,1,0:T(4,128)(2,1)} %reshape_reshape.3), calls=%async_computation | async-start | bytes 262144 | tf_op jit(solution)/shard_map/all_to_all | solution.py:114
  43.4 3.5 %copy-start.1 = (bf16[2048,1024]{1,0:T(8,128)(2,1)S(1)}, bf16[2048,1024]{1,0:T(8,128)(2,1)}, u32[]{:S(2)}) copy-start(bf16[2048,1024]{1,0:T(8,128)(2,1)} %param.34) | copy-start | bytes 12582916
  43.4 9.7 %copy-start.2 = (bf16[4096,512]{1,0:T(8,128)(2,1)S(1)}, bf16[4096,512]{1,0:T(8,128)(2,1)}, u32[]{:S(2)}) copy-start(bf16[4096,512]{1,0:T(8,128)(2,1)} %param.35) | copy-start | bytes 12582916
  46.8 10.9 %copy-start.3 = (f32[8,1,16384]{2,1,0:T(1,128)S(1)}, f32[8,1,16384]{2,1,0:T(1,128)}, u32[]{:S(2)}) copy-start(f32[8,1,16384]{2,1,0:T(1,128)} %param.27) | copy-start | bytes 1572868
  54.4 10.0 %all-to-all-start.1 = ((bf16[8,3,512]{2,1,0:T(4,128)(2,1)}), bf16[8,3,512]{2,1,0:T(4,128)(2,1)S(1)}, u32[]{:S(2)}, u32[]{:S(2)}) async-start(bf16[8,3,512]{2,1,0:T(4,128)(2,1)} %convert_element_type.100), calls=%async_computation.1 | async-start | bytes 65536 | tf_op jit(solution)/shard_map/all_to_all | solution.py:124
where the time goes:
time: 65.9 us; the launch traced here: 65.1 us
  blocking collectives  18.5 us (28%)
  matrix products  12.9 us (20%)
  waiting for transfers between devices  11.8 us (18%)
  starting transfers between devices  9.14 us (14%)
  other arithmetic  7.75 us (12%)
  local copies, waits for them, and re-layouts  4.36 us (7%)
  between operations  0.72 us (1%)
    psum x1, blocking collectives, shards(): lax.psum(partial_value.astype(jnp.bfloat16), 'tp').astype(jnp.float32)  12.9 us
    all_to_all x1, waiting for transfers between devices, shards(): lax.all_to_all(outbound, 'ep', split_axis=0, concat_axis=0, tiled=True)  7.14 us
    all_to_all x1, starting transfers between devices, shards(): lax.all_to_all(outbound, 'ep', split_axis=0, concat_axis=0, tiled=True)  5.8 us
    all_gather x1, blocking collectives, shards(): lax.all_gather(hidden, 'tp', axis=1, tiled=True)  5.59 us
    all_to_all x1, waiting for transfers between devices, shards(): lax.all_to_all(partial_out.reshape(sources, item_count, w_down.shape[1])....  4.63 us
    dot_general x3, matrix products, project(): product = jnp.dot(normed, weight, preferred_element_type=jnp.float32)  3.89 us
    all_to_all x1, starting transfers between devices, shards(): lax.all_to_all(partial_out.reshape(sources, item_count, w_down.shape[1])....  3.33 us
    dot_general x1, matrix products, shards(): gate_sum = jnp.dot(flat_rows, w_gate, preferred_element_type=jnp.float32)  2.99 us
  transfers between devices with their start and end apart: 2, of which 2 were waited for; matrix products, arithmetic and copies ran while one was open for 3% of the time, Pallas kernels for 0%

commit v1 on v0

v1 whole, which is shorter than its diff:
```python
import functools

import jax
import jax.numpy as jnp
from jax import lax
from jax.experimental import pallas as pl
from jax.experimental.pallas import tpu as pltpu
from jax.sharding import PartitionSpec as P

FF = 4096
epsilon = 1e-06
MESH = pl.DeviceIdType.MESH
F32 = jnp.float32
BF16 = jnp.bfloat16


def normalized(rows, gain):
    squares = jnp.sum(rows * rows, axis=1, keepdims=True) / rows.shape[1]
    return (rows * lax.rsqrt(squares + epsilon) * gain).astype(BF16)


def merged(ref, count):
    return jnp.concatenate([ref[i].astype(F32) for i in range(count)], axis=0)


def kernel(
    sizes,
    tokens,
    mix_gain,
    igate_rows,
    fgate_rows,
    forget_bias,
    norm_state,
    max_row,
    ffn_gain,
    ids,
    route_w,
    w_query,
    w_key,
    w_value,
    w_out,
    mem_state,
    w_gate,
    w_up,
    w_down,
    out_tokens,
    new_memory,
    new_norm,
    new_max_row,
    qkv_buf,
    out_buf,
    mem_buf,
    gate_buf,
    up_buf,
    down_buf,
    parts,
    residual_buf,
    packed,
    arrived,
    hidden_all,
    back,
    returned,
    load_sem,
    mem_sem,
    part_send,
    part_recv,
    row_send,
    row_recv,
    hid_send,
    hid_recv,
    back_send,
    back_recv,
):
    tp_count, ep_count, span, experts, slots, heads = sizes
    tp_at = lax.axis_index("tp")
    ep_at = lax.axis_index("ep")
    seqs, width = tokens.shape
    head_dim = mem_buf.shape[-1]
    own_width = out_tokens.shape[1]

    def load(src, dst, at):
        copy = pltpu.make_async_copy(src, dst, load_sem.at[at])
        copy.start()
        return copy

    loads = [load(w, qkv_buf.at[i], i) for i, w in enumerate((w_query, w_key, w_value))]
    load_mem = load(mem_state, mem_buf, 3)
    load_out = load(w_out, out_buf, 4)
    load_gate = load(w_gate, gate_buf, 5)
    load_up = load(w_up, up_buf, 6)
    load_down = load(w_down, down_buf, 7)

    barrier = pltpu.get_barrier_semaphore()
    for k in range(1, tp_count):
        pl.semaphore_signal(
            barrier, inc=1, device_id=(ep_at, lax.rem(tp_at + k, tp_count)), device_id_type=MESH
        )
    for k in range(1, ep_count):
        pl.semaphore_signal(
            barrier, inc=1, device_id=(lax.rem(ep_at + k, ep_count), tp_at), device_id_type=MESH
        )

    residual_in = tokens[...].astype(F32)
    normed = normalized(residual_in, mix_gain[...])

    def eye(n):
        return lax.broadcasted_iota(jnp.int32, (n, n), 0) == lax.broadcasted_iota(
            jnp.int32, (n, n), 1
        )

    def column(row):
        return jnp.sum(jnp.where(eye(seqs), row, jnp.zeros_like(row)), axis=1, keepdims=True)

    def row_of(col):
        return jnp.sum(jnp.where(eye(seqs), col, jnp.zeros_like(col)), axis=0, keepdims=True)

    contract = (((1,), (1,)), ((), ()))
    gates_i = lax.dot_general(normed, igate_rows[...], contract, preferred_element_type=F32)
    gates_f = lax.dot_general(normed, fgate_rows[...], contract, preferred_element_type=F32)
    lane = lax.broadcasted_iota(jnp.int32, gates_i.shape, 1)

    def slot_masks(shape, dim, group):
        at = lax.broadcasted_iota(jnp.int32, shape, dim)
        return at // group // slots, at % slots

    id0, id1 = ids[0:1, :], ids[1:2, :]
    expert_r, slot_r = slot_masks((experts * slots, seqs), 0, 1)
    match_r = jnp.where((id0 == expert_r) | (id1 == expert_r), 1.0, 0.0)
    before = lax.broadcasted_iota(jnp.int32, (seqs, seqs), 0) < lax.broadcasted_iota(
        jnp.int32, (seqs, seqs), 1
    )
    rank_r = jnp.dot(match_r, jnp.where(before, 1.0, 0.0), preferred_element_type=F32)
    placing = jnp.where(rank_r == slot_r.astype(F32), match_r, 0.0).astype(BF16)
    id0c, id1c = column(id0), column(id1)
    w0c, w1c = column(route_w[0:1, :]), column(route_w[1:2, :])
    at_c = lax.broadcasted_iota(jnp.int32, (seqs, ep_count * slots), 1)
    expert_c, slot_c = at_c // (slots * span), at_c % slots
    first, second = id0c == expert_c, id1c == expert_c
    match_c = jnp.where(first | second, 1.0, 0.0)
    after = lax.broadcasted_iota(jnp.int32, (seqs, seqs), 0) > lax.broadcasted_iota(
        jnp.int32, (seqs, seqs), 1
    )
    rank_c = jnp.dot(jnp.where(after, 1.0, 0.0), match_c, preferred_element_type=F32)
    mixing = jnp.where(
        rank_c == slot_c.astype(F32),
        jnp.where(first, w0c, 0.0) + jnp.where(second, w1c, 0.0),
        0.0,
    )

    for copy in loads:
        copy.wait()
    projected = [
        jnp.dot(normed, qkv_buf[i], preferred_element_type=F32).astype(BF16).astype(F32)
        for i in range(3)
    ]
    load_mem.wait()
    readouts, maxes = [], []
    for h in range(heads):
        at = tp_at * heads + h
        cut = slice(h * head_dim, (h + 1) * head_dim)
        query, value = projected[0][:, cut], projected[2][:, cut]
        key = projected[1][:, cut] * head_dim ** (-0.5)
        input_gate = jnp.sum(jnp.where(lane == at, gates_i, 0.0), axis=1, keepdims=True)
        pre = jnp.sum(jnp.where(lane == at, gates_f, 0.0), axis=1, keepdims=True) + forget_bias[at]
        forget_log = jnp.minimum(pre, 0.0) - jnp.log1p(jnp.exp(-jnp.abs(pre)))
        held = forget_log + column(max_row[h : h + 1, :])
        top = jnp.maximum(held, input_gate)
        keep = jnp.exp(held - top)
        fresh = jnp.exp(input_gate - top)
        new_max_row[h : h + 1, :] = row_of(top)
        norm = keep * norm_state[:, cut] + fresh * key
        new_norm[:, cut] = norm
        under = jnp.sum(query * norm, axis=1, keepdims=True)
        scaled = fresh * key
        pad = jnp.zeros((head_dim - 2 * seqs, head_dim), F32)
        turned = jnp.transpose(jnp.concatenate([scaled, query, pad], axis=0))
        over = []
        for s in range(seqs):
            cell = keep[s : s + 1, :] * mem_buf[s, h] + turned[:, s : s + 1] * value[s : s + 1, :]
            mem_buf[s, h] = cell
            over.append(jnp.sum(turned[:, seqs + s : seqs + s + 1] * cell, axis=0, keepdims=True))
        over = jnp.concatenate(over, axis=0)
        readouts.append((over / jnp.maximum(jnp.abs(under), jnp.exp(-top))).astype(BF16))
    readout = readouts[0] if heads == 1 else jnp.concatenate(readouts, axis=1)
    load_out.wait()
    parts[tp_at] = jnp.dot(readout, out_buf[...], preferred_element_type=F32).astype(BF16)
    pl.semaphore_wait(barrier, tp_count - 1 + ep_count - 1)

    def send(src, dst, sems, recvs, k, device):
        copy = pltpu.make_async_remote_copy(
            src_ref=src,
            dst_ref=dst,
            send_sem=sems.at[k],
            recv_sem=recvs.at[k],
            device_id=device,
            device_id_type=MESH,
        )
        copy.start()
        return copy

    sent = []
    part_copies = [
        send(
            parts.at[tp_at],
            parts.at[tp_at],
            part_send,
            part_recv,
            k,
            (ep_at, lax.rem(tp_at + k, tp_count)),
        )
        for k in range(1, tp_count)
    ]
    store_mem = pltpu.make_async_copy(mem_buf, new_memory, mem_sem)
    store_mem.start()
    for copy in part_copies:
        copy.wait_recv()
    sent += part_copies
    head_total = parts[0].astype(F32)
    for t in range(1, tp_count):
        head_total = head_total + parts[t].astype(F32)
    residual = (residual_in + head_total).astype(BF16).astype(F32)
    residual_buf[...] = residual
    outgoing = normalized(residual, ffn_gain[...])
    rows = jnp.dot(placing, outgoing, preferred_element_type=F32)
    for e in range(experts):
        packed[e] = rows[e * slots : (e + 1) * slots, :].astype(BF16)
    row_copies = []
    for k in range(1, ep_count):
        to = lax.rem(ep_at + k, ep_count)
        row_copies.append(
            send(packed.at[to // span], arrived.at[ep_at], row_send, row_recv, k, (to, tp_at))
        )
    arrived[ep_at] = packed[ep_at // span]
    load_gate.wait()
    load_up.wait()
    for copy in row_copies:
        copy.wait_recv()
    sent += row_copies
    flat = merged(arrived, ep_count).astype(BF16)
    units = gate_buf.shape[1]
    step = min(256, units)
    for at in range(0, units, step):
        gate = jnp.dot(flat, gate_buf[:, at : at + step], preferred_element_type=F32)
        up = jnp.dot(flat, up_buf[:, at : at + step], preferred_element_type=F32)
        hidden_all[tp_at, :, at : at + step] = (gate * jax.nn.sigmoid(gate) * up).astype(BF16)
    hid_copies = [
        send(
            hidden_all.at[tp_at],
            hidden_all.at[tp_at],
            hid_send,
            hid_recv,
            k,
            (ep_at, lax.rem(tp_at + k, tp_count)),
        )
        for k in range(1, tp_count)
    ]
    load_down.wait()
    total = None
    for k in range(tp_count):
        if k:
            hid_copies[k - 1].wait_recv()
        source = lax.rem(tp_at - k + tp_count, tp_count)
        start = pl.multiple_of(source * units, units)
        term = jnp.dot(
            hidden_all[source], down_buf[pl.ds(start, units), :], preferred_element_type=F32
        )
        total = term if total is None else total + term
    sent += hid_copies
    for i in range(ep_count):
        back[i] = total[i * slots : (i + 1) * slots, :].astype(BF16)
    back_copies = []
    for k in range(1, ep_count):
        to = lax.rem(ep_at + k, ep_count)
        back_copies.append(
            send(back.at[to], returned.at[ep_at], back_send, back_recv, k, (to, tp_at))
        )
    returned[ep_at] = back[ep_at]
    for copy in back_copies:
        copy.wait_recv()
    sent += back_copies
    results = merged(returned, ep_count)
    routed = jnp.dot(
        mixing, results, precision=lax.Precision.HIGHEST, preferred_element_type=F32
    )
    own = residual_buf[:, pl.ds(pl.multiple_of(tp_at * own_width, own_width), own_width)]
    out_tokens[...] = (own + routed).astype(BF16)
    for copy in sent:
        copy.wait_send()
    store_mem.wait()


def shards(
    tokens,
    mix_gain,
    w_query,
    w_key,
    w_value,
    w_igate,
    w_fgate,
    forget_bias,
    w_out,
    mem_state,
    norm_state,
    max_state,
    ffn_gain,
    route_ids,
    route_weights,
    w_gate,
    w_up,
    w_down,
):
    seqs, width = tokens.shape
    heads = mem_state.shape[1]
    head_dim = norm_state.shape[1] // heads
    tp_count = lax.axis_size("tp")
    ep_count = lax.axis_size("ep")
    own_width = width // tp_count
    top_count = route_ids.shape[1]
    span = FF // w_down.shape[0]
    experts = ep_count // span
    slot_cap = max(2, 3 * seqs * top_count // (2 * experts))
    slots = -(-slot_cap // 4) * 4
    memory = mem_state.reshape(seqs, heads, head_dim, head_dim)
    total = ep_count * slots
    units = w_gate.shape[1]
    vmem = pl.BlockSpec(memory_space=pltpu.VMEM)
    smem = pl.BlockSpec(memory_space=pltpu.SMEM)
    hbm = pl.BlockSpec(memory_space=pl.ANY)
    dma = pltpu.SemaphoreType.DMA
    outs = pl.pallas_call(
        functools.partial(kernel, (tp_count, ep_count, span, experts, slots, heads)),
        out_shape=(
            jax.ShapeDtypeStruct((seqs, own_width), BF16),
            jax.ShapeDtypeStruct(memory.shape, F32),
            jax.ShapeDtypeStruct(norm_state.shape, F32),
            jax.ShapeDtypeStruct((heads, seqs), F32),
        ),
        in_specs=[vmem] * 4 + [smem] + [vmem] * 5 + [hbm] * 8,
        out_specs=(vmem, hbm, vmem, vmem),
        scratch_shapes=[
            pltpu.VMEM((3,) + w_query.shape, BF16),
            pltpu.VMEM(w_out.shape, BF16),
            pltpu.VMEM(memory.shape, F32),
            pltpu.VMEM(w_gate.shape, BF16),
            pltpu.VMEM(w_up.shape, BF16),
            pltpu.VMEM(w_down.shape, BF16),
            pltpu.VMEM((tp_count, seqs, width), BF16),
            pltpu.VMEM((seqs, width), F32),
            pltpu.VMEM((experts, slots, width), BF16),
            pltpu.VMEM((ep_count, slots, width), BF16),
            pltpu.VMEM((tp_count, total, units), BF16),
            pltpu.VMEM((ep_count, slots, own_width), BF16),
            pltpu.VMEM((ep_count, slots, own_width), BF16),
            dma((8,)),
            dma,
            dma((tp_count,)),
            dma((tp_count,)),
            dma((ep_count,)),
            dma((ep_count,)),
            dma((tp_count,)),
            dma((tp_count,)),
            dma((ep_count,)),
            dma((ep_count,)),
        ],
        compiler_params=pltpu.CompilerParams(
            collective_id=0, has_side_effects=True, vmem_limit_bytes=60 * 1024 * 1024
        ),
    )(
        tokens,
        mix_gain.astype(F32).reshape(1, width),
        w_igate.T,
        w_fgate.T,
        forget_bias,
        norm_state,
        max_state.T,
        ffn_gain.astype(F32).reshape(1, width),
        route_ids.T,
        route_weights.T,
        w_query,
        w_key,
        w_value,
        w_out,
        memory,
        w_gate,
        w_up,
        w_down,
    )
    return outs[0], outs[1].reshape(mem_state.shape), outs[2], outs[3].T


def solution(mesh):
    placed = (
        P("ep", None),
        P(),
        P(None, "tp"),
        P(None, "tp"),
        P(None, "tp"),
        P(),
        P(),
        P(),
        P("tp", None),
        P("ep", "tp", None),
        P("ep", "tp"),
        P("ep", "tp"),
        P(),
        P("ep", None),
        P("ep", None),
        P(None, ("ep", "tp")),
        P(None, ("ep", "tp")),
        P("ep", "tp"),
    )
    return jax.shard_map(
        shards,
        mesh=mesh,
        in_specs=placed,
        out_specs=(P("ep", "tp"), P("ep", "tp", None), P("ep", "tp"), P("ep", "tp")),
        check_vma=False,
    )
```

time: 65.9 us -> 35.3 us (0.54)
  Pallas kernels: 0 us -> 26.1 us
  blocking collectives: 18.5 us -> 0 us
  matrix products: 12.9 us -> 0 us
  waiting for transfers between devices: 11.8 us -> 0 us
  starting transfers between devices: 9.14 us -> 0 us
  other arithmetic: 7.75 us -> 2.57 us
  local copies, waits for them, and re-layouts: 4.36 us -> 5.59 us
    pallas_call x0 -> x1, Pallas kernels: none -> 26.1 us  [shards(): pl.pallas_call(functools.partial(kernel, (tp_count, ep_count, span, exper...]
    psum x1 -> x0, blocking collectives: 12.9 us -> none  [shards(): lax.psum(partial_value.astype(jnp.bfloat16), 'tp').astype(jnp.float32)]
    dot_general x12 -> x0, matrix products: 12.9 us -> none  [the longest x3 3.89 us: project(): product = jnp.dot(normed, weight, preferred_element_type=jnp.float32)]
    all_to_all x2 -> x0, waiting for transfers between devices: 11.8 us -> none  [the longest x1 7.14 us: shards(): lax.all_to_all(outbound, 'ep', split_axis=0, concat_axis=0, tiled=True)]
    all_to_all x2 -> x0, starting transfers between devices: 9.14 us -> none  [the longest x1 5.8 us: shards(): lax.all_to_all(outbound, 'ep', split_axis=0, concat_axis=0, tiled=True)]
    all_gather x1 -> x0, blocking collectives: 5.59 us -> none  [shards(): lax.all_gather(hidden, 'tp', axis=1, tiled=True)]
    reduce_sum x5 -> x0, other arithmetic: 3.49 us -> none  [the longest x1 1.47 us: shards(): denominator = jnp.sum(query_rows * new_norm, axis=2)]
    unnamed x11 -> x4, local copies, waits for them, and re-layouts: 2.53 us -> 5.59 us
  transfers between devices with their start and end apart: 2 -> 0, of which waited for: 2 -> 0; matrix products, arithmetic and copies ran while one was open for 3% -> 0% of each run, Pallas kernels for 0% -> 0%
where the time goes in v1:
time: 35.3 us; the launch traced here: 34.9 us
  Pallas kernels  26.1 us (74%)
  local copies, waits for them, and re-layouts  5.59 us (16%)
  other arithmetic  2.57 us (7%)
  between operations  0.64 us (2%)
    pallas_call x1, Pallas kernels, shards(): pl.pallas_call(functools.partial(kernel, (tp_count, ep_count, span, exper...  26.1 us
    unnamed x4, local copies, waits for them, and re-layouts  5.59 us
    reshape x1, other arithmetic, shards(): mix_gain.astype(F32).reshape(1, width)  1.29 us
    reshape x1, other arithmetic, shards(): ffn_gain.astype(F32).reshape(1, width)  1.29 us

profile of v1, /device:TPU:0, one launch (start us, length us, event | category | flops | bytes accessed | tf_op | source)
XLA Modules:
  0.0 34.9 jit_solution(14466216669893935645)
XLA Ops:
  0.6 1.3 %reshape.30 = f32[2048]{0:T(1024)} convert(bf16[2048]{0:T(1024)(128)(2,1)} %param.19) | non-fusion elementwise | flops 2048 | bytes 12288 | tf_op jit(solution)/shard_map/reshape | solution.py:370
  1.9 1.3 %reshape.32 = f32[2048]{0:T(1024)} convert(bf16[2048]{0:T(1024)(128)(2,1)} %param.30) | non-fusion elementwise | flops 2048 | bytes 12288 | tf_op jit(solution)/shard_map/reshape | solution.py:376
  3.2 26.1 %shard_map.201 = (bf16[8,512]{1,0:T(8,128)(2,1)}, f32[8,1,128,128]{3,2,1,0:T(8,128)}, f32[8,128]{1,0:T(8,128)}, f32[1,8]{1,0:T(1,128)}) custom-call(bf16[8,2048]{1,0:T(8,128)(2,1)} %tokens.1, f32[1,2048]{1,0:T(1,128)} %bitcast.12, bf16[4,2048]{1,0:T(4,128)(2,1)} %bitcast.14, bf16[4,2048]{1,0:T(4,128)(2,1)} %bitcast.15, f32[4]{0:T(128)} %forget_bias.1, ...), custom_call_target="tpu_custom_call" | custom-call | tf_op jit(solution)/shard_map/pallas_call | solution.py:330
  29.3 1.3 %copy.27 = bf16[8,512]{1,0:T(8,128)(2,1)} copy(bf16[8,512]{1,0:T(8,128)(2,1)} %get-tuple-element.20) | data formatting | bytes 16384
  30.6 1.9 %copy.28 = f32[8,1,16384]{2,1,0:T(1,128)} copy(f32[8,1,16384]{2,1,0:T(1,128)} %bitcast.11) | data formatting | bytes 1048576
  32.5 1.3 %copy.29 = f32[8,128]{1,0:T(8,128)} copy(f32[8,128]{1,0:T(8,128)} %get-tuple-element.22) | data formatting | bytes 8192
  33.8 1.1 %copy.30 = f32[8,1]{0,1:T(1,128)} copy(f32[8,1]{0,1:T(1,128)} %bitcast.19) | data formatting | bytes 64

commit v2 on v1

--- a/solution.py
+++ b/solution.py
@@ -101,7 +101,7 @@
         )
 
     residual_in = tokens[...].astype(F32)
-    normed = normalized(residual_in, mix_gain[...])
+    normed = normalized(residual_in, mix_gain[...].astype(F32).reshape(1, width))
 
     def eye(n):
         return lax.broadcasted_iota(jnp.int32, (n, n), 0) == lax.broadcasted_iota(
@@ -220,7 +220,7 @@
         head_total = head_total + parts[t].astype(F32)
     residual = (residual_in + head_total).astype(BF16).astype(F32)
     residual_buf[...] = residual
-    outgoing = normalized(residual, ffn_gain[...])
+    outgoing = normalized(residual, ffn_gain[...].astype(F32).reshape(1, width))
     rows = jnp.dot(placing, outgoing, preferred_element_type=F32)
     for e in range(experts):
         packed[e] = rows[e * slots : (e + 1) * slots, :].astype(BF16)
@@ -287,6 +287,24 @@
     for copy in sent:
         copy.wait_send()
     store_mem.wait()
+
+
+def hand_on(count, *refs):
+    sources, targets, held = refs[:count], refs[count : 2 * count], refs[2 * count : 3 * count]
+    in_sem, out_sem = refs[3 * count :]
+    reads = [
+        pltpu.make_async_copy(sources[i], held[i], in_sem.at[i]) for i in range(count)
+    ]
+    writes = [
+        pltpu.make_async_copy(held[i], targets[i], out_sem.at[i]) for i in range(count)
+    ]
+    for copy in reads:
+        copy.start()
+    for read, write in zip(reads, writes):
+        read.wait()
+        write.start()
+    for copy in writes:
+        copy.wait()
 
 
 def shards(
@@ -367,13 +385,13 @@
         ),
     )(
         tokens,
-        mix_gain.astype(F32).reshape(1, width),
+        mix_gain,
         w_igate.T,
         w_fgate.T,
         forget_bias,
         norm_state,
         max_state.T,
-        ffn_gain.astype(F32).reshape(1, width),
+        ffn_gain,
         route_ids.T,
         route_weights.T,
         w_query,
@@ -385,6 +403,15 @@
         w_up,
         w_down,
     )
+    outs = pl.pallas_call(
+        functools.partial(hand_on, len(outs)),
+        out_shape=tuple(jax.ShapeDtypeStruct(o.shape, o.dtype) for o in outs),
+        in_specs=[hbm] * len(outs),
+        out_specs=(hbm,) * len(outs),
+        scratch_shapes=[pltpu.VMEM(o.shape, o.dtype) for o in outs]
+        + [dma((len(outs),)), dma((len(outs),))],
+        compiler_params=pltpu.CompilerParams(vmem_limit_bytes=60 * 1024 * 1024),
+    )(*outs)
     return outs[0], outs[1].reshape(mem_state.shape), outs[2], outs[3].T
 
 

time: 35.3 us -> 28.9 us (0.82)
  local copies, waits for them, and re-layouts: 5.59 us -> 0 us
  other arithmetic: 2.57 us -> 0 us
  Pallas kernels: 26.1 us -> 28.1 us
    unnamed x4 -> x0, local copies, waits for them, and re-layouts: 5.59 us -> none
    reshape x2 -> x0, other arithmetic: 2.57 us -> none  [the longest x1 1.29 us: shards(): mix_gain.astype(F32).reshape(1, width)]
    pallas_call x0 -> x1, Pallas kernels: none -> 1.93 us  [shards(): pl.pallas_call(functools.partial(hand_on, len(outs)), out_shape=tuple((ja...]
where the time goes in v2:
time: 28.9 us; the launch traced here: 28.7 us
  Pallas kernels  28.1 us (97%)
  between operations  0.65 us (2%)
    pallas_call x1, Pallas kernels, shards(): pl.pallas_call(functools.partial(kernel, (tp_count, ep_count, span, exper...  26.2 us
    pallas_call x1, Pallas kernels, shards(): pl.pallas_call(functools.partial(hand_on, len(outs)), out_shape=tuple((ja...  1.93 us

profile of v2, /device:TPU:0, one launch (start us, length us, event | category | flops | bytes accessed | tf_op | source)
XLA Modules:
  0.0 28.7 jit_solution(10791515535138379172)
XLA Ops:
  0.6 26.2 %shard_map.201 = (bf16[8,512]{1,0:T(8,128)(2,1)}, f32[8,1,128,128]{3,2,1,0:T(8,128)}, f32[8,128]{1,0:T(8,128)}, f32[1,8]{1,0:T(1,128)}) custom-call(bf16[8,2048]{1,0:T(8,128)(2,1)} %tokens.1, bf16[2048]{0:T(1024)(128)(2,1)} %mix_gain.1, bf16[4,2048]{1,0:T(4,128)(2,1)} %bitcast.9, bf16[4,2048]{1,0:T(4,128)(2,1)} %bitcast.10, f32[4]{0:T(128)} %forget_bias.1, ...), custom_call_target="tpu_custom_call" | custom-call | tf_op jit(solution)/shard_map/pallas_call | solution.py:348
  26.8 1.9 %shard_map.202 = (bf16[8,512]{1,0:T(8,128)(2,1)}, f32[8,1,128,128]{3,2,1,0:T(8,128)}, f32[8,128]{1,0:T(8,128)}, f32[1,8]{1,0:T(1,128)}) custom-call(bf16[8,512]{1,0:T(8,128)(2,1)} %get-tuple-element.12.refs_0_, f32[8,1,128,128]{3,2,1,0:T(8,128)} %get-tuple-element.13.refs_1_, f32[8,128]{1,0:T(8,128)} %get-tuple-element.14.refs_2_, ...), custom_call_target="tpu_custom_call" | custom-call | tf_op jit(solution)/shard_map/pallas_call | solution.py:406

commit v3 on v1

--- a/solution.py
+++ b/solution.py
@@ -49,7 +49,6 @@
     new_max_row,
     qkv_buf,
     out_buf,
-    mem_buf,
     gate_buf,
     up_buf,
     down_buf,
@@ -61,7 +60,6 @@
     back,
     returned,
     load_sem,
-    mem_sem,
     part_send,
     part_recv,
     row_send,
@@ -75,7 +73,7 @@
     tp_at = lax.axis_index("tp")
     ep_at = lax.axis_index("ep")
     seqs, width = tokens.shape
-    head_dim = mem_buf.shape[-1]
+    head_dim = new_memory.shape[-1]
     own_width = out_tokens.shape[1]
 
     def load(src, dst, at):
@@ -84,7 +82,7 @@
         return copy
 
     loads = [load(w, qkv_buf.at[i], i) for i, w in enumerate((w_query, w_key, w_value))]
-    load_mem = load(mem_state, mem_buf, 3)
+    load_mem = load(mem_state, new_memory, 3)
     load_out = load(w_out, out_buf, 4)
     load_gate = load(w_gate, gate_buf, 5)
     load_up = load(w_up, up_buf, 6)
@@ -101,7 +99,7 @@
         )
 
     residual_in = tokens[...].astype(F32)
-    normed = normalized(residual_in, mix_gain[...])
+    normed = normalized(residual_in, mix_gain[...].astype(F32).reshape(1, width))
 
     def eye(n):
         return lax.broadcasted_iota(jnp.int32, (n, n), 0) == lax.broadcasted_iota(
@@ -176,8 +174,8 @@
         turned = jnp.transpose(jnp.concatenate([scaled, query, pad], axis=0))
         over = []
         for s in range(seqs):
-            cell = keep[s : s + 1, :] * mem_buf[s, h] + turned[:, s : s + 1] * value[s : s + 1, :]
-            mem_buf[s, h] = cell
+            cell = keep[s : s + 1, :] * new_memory[s, h] + turned[:, s : s + 1] * value[s : s + 1, :]
+            new_memory[s, h] = cell
             over.append(jnp.sum(turned[:, seqs + s : seqs + s + 1] * cell, axis=0, keepdims=True))
         over = jnp.concatenate(over, axis=0)
         readouts.append((over / jnp.maximum(jnp.abs(under), jnp.exp(-top))).astype(BF16))
@@ -210,8 +208,6 @@
         )
         for k in range(1, tp_count)
     ]
-    store_mem = pltpu.make_async_copy(mem_buf, new_memory, mem_sem)
-    store_mem.start()
     for copy in part_copies:
         copy.wait_recv()
     sent += part_copies
@@ -220,7 +216,7 @@
         head_total = head_total + parts[t].astype(F32)
     residual = (residual_in + head_total).astype(BF16).astype(F32)
     residual_buf[...] = residual
-    outgoing = normalized(residual, ffn_gain[...])
+    outgoing = normalized(residual, ffn_gain[...].astype(F32).reshape(1, width))
     rows = jnp.dot(placing, outgoing, preferred_element_type=F32)
     for e in range(experts):
         packed[e] = rows[e * slots : (e + 1) * slots, :].astype(BF16)
@@ -238,33 +234,36 @@
     sent += row_copies
     flat = merged(arrived, ep_count).astype(BF16)
     units = gate_buf.shape[1]
-    step = min(256, units)
-    for at in range(0, units, step):
-        gate = jnp.dot(flat, gate_buf[:, at : at + step], preferred_element_type=F32)
-        up = jnp.dot(flat, up_buf[:, at : at + step], preferred_element_type=F32)
-        hidden_all[tp_at, :, at : at + step] = (gate * jax.nn.sigmoid(gate) * up).astype(BF16)
-    hid_copies = [
-        send(
-            hidden_all.at[tp_at],
-            hidden_all.at[tp_at],
-            hid_send,
-            hid_recv,
-            k,
-            (ep_at, lax.rem(tp_at + k, tp_count)),
-        )
-        for k in range(1, tp_count)
-    ]
+    chunks, step = hidden_all.shape[1], hidden_all.shape[3]
+    hid_copies = {}
+    for c in range(chunks):
+        cut = slice(c * step, (c + 1) * step)
+        gate = jnp.dot(flat, gate_buf[:, cut], preferred_element_type=F32)
+        up = jnp.dot(flat, up_buf[:, cut], preferred_element_type=F32)
+        hidden_all[tp_at, c] = (gate * jax.nn.sigmoid(gate) * up).astype(BF16)
+        for k in range(1, tp_count):
+            hid_copies[k, c] = send(
+                hidden_all.at[tp_at, c],
+                hidden_all.at[tp_at, c],
+                hid_send,
+                hid_recv,
+                k * chunks + c,
+                (ep_at, lax.rem(tp_at + k, tp_count)),
+            )
     load_down.wait()
     total = None
-    for k in range(tp_count):
+    for k, c in [(0, c) for c in range(chunks)] + [
+        (k, c) for c in range(chunks) for k in range(1, tp_count)
+    ]:
         if k:
-            hid_copies[k - 1].wait_recv()
+            hid_copies[k, c].wait_recv()
         source = lax.rem(tp_at - k + tp_count, tp_count)
-        start = pl.multiple_of(source * units, units)
+        start = pl.multiple_of(source * units + c * step, step)
         term = jnp.dot(
-            hidden_all[source], down_buf[pl.ds(start, units), :], preferred_element_type=F32
+            hidden_all[source, c], down_buf[pl.ds(start, step), :], preferred_element_type=F32
         )
         total = term if total is None else total + term
+    hid_copies = list(hid_copies.values())
     sent += hid_copies
     for i in range(ep_count):
         back[i] = total[i * slots : (i + 1) * slots, :].astype(BF16)
@@ -286,7 +285,17 @@
     out_tokens[...] = (own + routed).astype(BF16)
     for copy in sent:
         copy.wait_send()
-    store_mem.wait()
+
+
+def hand_on(count, *refs):
+    sems = refs[2 * count]
+    copies = [
+        pltpu.make_async_copy(refs[i], refs[count + i], sems.at[i]) for i in range(count)
+    ]
+    for copy in copies:
+        copy.start()
+    for copy in copies:
+        copy.wait()
 
 
 def shards(
@@ -319,28 +328,27 @@
     span = FF // w_down.shape[0]
     experts = ep_count // span
     slot_cap = max(2, 3 * seqs * top_count // (2 * experts))
-    slots = -(-slot_cap // 4) * 4
+    slots = slot_cap
     memory = mem_state.reshape(seqs, heads, head_dim, head_dim)
     total = ep_count * slots
     units = w_gate.shape[1]
+    step = min(256, units)
     vmem = pl.BlockSpec(memory_space=pltpu.VMEM)
     smem = pl.BlockSpec(memory_space=pltpu.SMEM)
-    hbm = pl.BlockSpec(memory_space=pl.ANY)
     dma = pltpu.SemaphoreType.DMA
     outs = pl.pallas_call(
         functools.partial(kernel, (tp_count, ep_count, span, experts, slots, heads)),
         out_shape=(
-            jax.ShapeDtypeStruct((seqs, own_width), BF16),
-            jax.ShapeDtypeStruct(memory.shape, F32),
-            jax.ShapeDtypeStruct(norm_state.shape, F32),
-            jax.ShapeDtypeStruct((heads, seqs), F32),
+            pltpu.VMEM((seqs, own_width), BF16),
+            pltpu.VMEM(memory.shape, F32),
+            pltpu.VMEM(norm_state.shape, F32),
+            pltpu.VMEM((heads, seqs), F32),
         ),
-        in_specs=[vmem] * 4 + [smem] + [vmem] * 5 + [hbm] * 8,
-        out_specs=(vmem, hbm, vmem, vmem),
+        in_specs=[vmem] * 4 + [smem] + [vmem] * 5 + [pl.BlockSpec(memory_space=pltpu.HBM)] * 8,
+        out_specs=(vmem,) * 4,
         scratch_shapes=[
             pltpu.VMEM((3,) + w_query.shape, BF16),
             pltpu.VMEM(w_out.shape, BF16),
-            pltpu.VMEM(memory.shape, F32),
             pltpu.VMEM(w_gate.shape, BF16),
             pltpu.VMEM(w_up.shape, BF16),
             pltpu.VMEM(w_down.shape, BF16),
@@ -348,32 +356,31 @@
             pltpu.VMEM((seqs, width), F32),
             pltpu.VMEM((experts, slots, width), BF16),
             pltpu.VMEM((ep_count, slots, width), BF16),
-            pltpu.VMEM((tp_count, total, units), BF16),
+            pltpu.VMEM((tp_count, units // step, total, step), BF16),
             pltpu.VMEM((ep_count, slots, own_width), BF16),
             pltpu.VMEM((ep_count, slots, own_width), BF16),
             dma((8,)),
-            dma,
             dma((tp_count,)),
             dma((tp_count,)),
             dma((ep_count,)),
             dma((ep_count,)),
-            dma((tp_count,)),
-            dma((tp_count,)),
+            dma((tp_count * (units // step),)),
+            dma((tp_count * (units // step),)),
             dma((ep_count,)),
             dma((ep_count,)),
         ],
         compiler_params=pltpu.CompilerParams(
-            collective_id=0, has_side_effects=True, vmem_limit_bytes=60 * 1024 * 1024
+            collective_id=0, has_side_effects=True, vmem_limit_bytes=67043328 - 600 * 1024
         ),
     )(
         tokens,
-        mix_gain.astype(F32).reshape(1, width),
+        mix_gain,
         w_igate.T,
         w_fgate.T,
         forget_bias,
         norm_state,
         max_state.T,
-        ffn_gain.astype(F32).reshape(1, width),
+        ffn_gain,
         route_ids.T,
         route_weights.T,
         w_query,
@@ -385,6 +392,14 @@
         w_up,
         w_down,
     )
+    outs = pl.pallas_call(
+        functools.partial(hand_on, len(outs)),
+        out_shape=tuple(jax.ShapeDtypeStruct(o.shape, o.dtype) for o in outs),
+        in_specs=[vmem] * len(outs),
+        out_specs=(pl.BlockSpec(memory_space=pltpu.HBM),) * len(outs),
+        scratch_shapes=[dma((len(outs),))],
+        compiler_params=pltpu.CompilerParams(vmem_limit_bytes=4 * 1024 * 1024),
+    )(*outs)
     return outs[0], outs[1].reshape(mem_state.shape), outs[2], outs[3].T
 
 

time: 35.3 us -> 27 us (0.76)
  local copies, waits for them, and re-layouts: 5.59 us -> 0 us
  other arithmetic: 2.57 us -> 0 us
    unnamed x4 -> x0, local copies, waits for them, and re-layouts: 5.59 us -> none
    reshape x2 -> x0, other arithmetic: 2.57 us -> none  [the longest x1 1.29 us: shards(): mix_gain.astype(F32).reshape(1, width)]
    pallas_call x0 -> x1, Pallas kernels: none -> 0.84 us  [shards(): pl.pallas_call(functools.partial(hand_on, len(outs)), out_shape=tuple((ja...]
    pallas_call x1, Pallas kernels: 26.1 us -> 25.3 us  [shards(): pl.pallas_call(functools.partial(kernel, (tp_count, ep_count, span, exper...]
where the time goes in v3:
time: 27 us; the launch traced here: 26.8 us
  Pallas kernels  26.2 us (97%)
  between operations  0.65 us (2%)
    pallas_call x1, Pallas kernels, shards(): pl.pallas_call(functools.partial(kernel, (tp_count, ep_count, span, exper...  25.3 us
    pallas_call x1, Pallas kernels, shards(): pl.pallas_call(functools.partial(hand_on, len(outs)), out_shape=tuple((ja...  0.84 us

profile of v3, /device:TPU:0, one launch (start us, length us, event | category | flops | bytes accessed | tf_op | source)
XLA Modules:
  0.0 26.8 jit_solution(15798561065632487780)
XLA Ops:
  0.6 25.3 %shard_map.201 = (bf16[8,512]{1,0:T(8,128)(2,1)S(1)}, f32[8,1,128,128]{3,2,1,0:T(8,128)S(1)}, f32[8,128]{1,0:T(8,128)S(1)}, f32[1,8]{1,0:T(1,128)S(1)}) custom-call(bf16[8,2048]{1,0:T(8,128)(2,1)} %tokens.1, bf16[2048]{0:T(1024)(128)(2,1)} %mix_gain.1, bf16[4,2048]{1,0:T(4,128)(2,1)} %bitcast.9, bf16[4,2048]{1,0:T(4,128)(2,1)} %bitcast.10, f32[4]{0:T(128)} %forget_bias.1, ...), custom_call_target="tpu_custom_call" | custom-call | tf_op jit(solution)/shard_map/pallas_call | solution.py:339
  26.0 0.8 %shard_map.202 = (bf16[8,512]{1,0:T(8,128)(2,1)}, f32[8,1,128,128]{3,2,1,0:T(8,128)}, f32[8,128]{1,0:T(8,128)}, f32[1,8]{1,0:T(1,128)}) custom-call(bf16[8,512]{1,0:T(8,128)(2,1)S(1)} %get-tuple-element.12.refs_0_, f32[8,1,128,128]{3,2,1,0:T(8,128)S(1)} %get-tuple-element.13.refs_1_, f32[8,128]{1,0:T(8,128)S(1)} %get-tuple-element.14.refs_2_, ...), custom_call_target="tpu_custom_call" | custom-call | tf_op jit(solution)/shard_map/pallas_call | solution.py:395
